TPU v7x, 32 devices: a whole 2x2x4 slice. The times are simulated.
32 devices in a mesh: fs: 8 (over z, y), tp: 4 (over x, core).
Axes of the slice: x: 2, y: 2, z: 4, core: 2. Of those that a mesh axis runs over, the one named last changes fastest.
Arguments:
- saved_inputs: bfloat16 [16384, 4096], P('fs'), may hold values from -6 to 6
- value_cot: bfloat16 [16384, 1024], P('fs', 'tp'), may hold values from -6 to 6
- gate_cot: bfloat16 [16384, 1024], P('fs', 'tp'), may hold values from -6 to 6
- point_inputs: bfloat16 [16384, 1024], P('fs'), may hold values from -6 to 6
- point_cot: bfloat16 [16384, 1024], P('fs', 'tp'), may hold values from -6 to 6
- master_value: float32 [4096, 1024], P('fs', 'tp'), may hold values from -6 to 6
- master_gate: float32 [4096, 1024], P('fs', 'tp'), may hold values from -6 to 6
- master_point: float32 [1024, 1024], P('fs', 'tp'), may hold values from -6 to 6
- factor_value: bfloat16 [4096, 256], P('fs'), may hold values from -160 to 160
- factor_gate: bfloat16 [4096, 256], P('fs'), may hold values from -160 to 160
- factor_point: bfloat16 [1024, 256], P('fs'), may hold values from -160 to 160
- first_value: float32 [256, 1024], P('fs', 'tp'), may hold values from -6 to 6
- first_gate: float32 [256, 1024], P('fs', 'tp'), may hold values from -6 to 6
- first_point: float32 [256, 1024], P('fs', 'tp'), may hold values from -6 to 6
- second_value: float32 [256, 1024], P('fs', 'tp'), may hold values from 0.2 to 2
- second_gate: float32 [256, 1024], P('fs', 'tp'), may hold values from 0.2 to 2
- second_point: float32 [256, 1024], P('fs', 'tp'), may hold values from 0.2 to 2
Outputs:
- new_value: float32 [4096, 1024], P('fs', 'tp')
- new_gate: float32 [4096, 1024], P('fs', 'tp')
- new_point: float32 [1024, 1024], P('fs', 'tp')
- copy_value: bfloat16 [4096, 1024], P(None, 'tp')
- copy_gate: bfloat16 [4096, 1024], P(None, 'tp')
- copy_point: bfloat16 [1024, 1024], P(None, 'tp')
- next_first_value: float32 [256, 1024], P('fs', 'tp')
- next_first_gate: float32 [256, 1024], P('fs', 'tp')
- next_first_point: float32 [256, 1024], P('fs', 'tp')
- next_second_value: float32 [256, 1024], P('fs', 'tp')
- next_second_gate: float32 [256, 1024], P('fs', 'tp')
- next_second_point: float32 [256, 1024], P('fs', 'tp')
All inputs are finite; a program needn't handle non-finite values.
Results may differ from a plain program's by a relative error of at most 0.0055.
Values may be sent and summed in bfloat16 or wider, within the bound.
A program may use at most 128 MiB of HBM per device.

v0:
```python
import jax
import jax.numpy as jnp
from jax import lax
from jax.sharding import PartitionSpec as P


def contract_rows(left, right):
    return lax.dot_general(
        left, right, (((0,), (0,)), ((), ())), preferred_element_type=jnp.float32
    )


def contract_split(projected, cot):
    upper = projected.astype(jnp.bfloat16)
    lower = (projected - upper.astype(jnp.float32)).astype(jnp.bfloat16)
    return contract_rows(upper, cot) + contract_rows(lower, cot)


def moments(low, first_old, second_old):
    first = 0.8 * first_old + 0.2 * low
    second = 0.9 * second_old + 0.1 * low * low
    return (first, second, first / (jnp.sqrt(second) + 1e-08))


def local(
    saved_inputs,
    value_cot,
    gate_cot,
    point_inputs,
    point_cot,
    master_value,
    master_gate,
    master_point,
    factor_value,
    factor_gate,
    factor_point,
    first_value,
    first_gate,
    first_point,
    second_value,
    second_gate,
    second_point,
):
    total = saved_inputs.shape[0] * lax.axis_size("fs")
    columns = saved_inputs
    proj_value = jnp.dot(
        columns,
        lax.all_gather(factor_value, "fs", axis=0, tiled=True),
        preferred_element_type=jnp.float32,
    )
    proj_gate = jnp.dot(
        columns,
        lax.all_gather(factor_gate, "fs", axis=0, tiled=True),
        preferred_element_type=jnp.float32,
    )
    columns = point_inputs
    proj_point = jnp.dot(
        columns,
        lax.all_gather(factor_point, "fs", axis=0, tiled=True),
        preferred_element_type=jnp.float32,
    )
    low_value = contract_split(proj_value, value_cot)
    low_gate = contract_split(proj_gate, gate_cot)
    low_point = contract_split(proj_point, point_cot)
    summed = (
        lax.psum_scatter(low_value, "fs", scatter_dimension=0, tiled=True),
        lax.psum_scatter(low_gate, "fs", scatter_dimension=0, tiled=True),
        lax.psum_scatter(low_point, "fs", scatter_dimension=0, tiled=True),
    )
    fv, sv, dv = moments(summed[0] / total, first_value, second_value)
    fg, sg, dg = moments(summed[1] / total, first_gate, second_gate)
    fpt, spt, dpt = moments(summed[2] / total, first_point, second_point)
    whole_v, whole_g, whole_p = (
        lax.all_gather(dv, "fs", axis=0, tiled=True),
        lax.all_gather(dg, "fs", axis=0, tiled=True),
        lax.all_gather(dpt, "fs", axis=0, tiled=True),
    )
    full_v = jnp.dot(factor_value.astype(jnp.float32), whole_v, precision=lax.Precision.HIGHEST)
    full_g = jnp.dot(factor_gate.astype(jnp.float32), whole_g, precision=lax.Precision.HIGHEST)
    full_p = jnp.dot(factor_point.astype(jnp.float32), whole_p, precision=lax.Precision.HIGHEST)
    squares = lax.psum(
        (jnp.sum(full_v * full_v), jnp.sum(full_g * full_g), jnp.sum(full_p * full_p)), ("fs", "tp")
    )
    spread = lax.axis_size("fs") * lax.axis_size("tp")
    entries_in = full_v.shape[0] * full_v.shape[1] * spread
    entries_point = full_p.shape[0] * full_p.shape[1] * spread
    new_v = master_value - 0.1 * lax.rsqrt(squares[0] / entries_in + 1e-06) * full_v
    new_g = master_gate - 0.1 * lax.rsqrt(squares[1] / entries_in + 1e-06) * full_g
    new_p = master_point - 0.1 * lax.rsqrt(squares[2] / entries_point + 1e-06) * full_p
    copy_v, copy_g, copy_p = (
        lax.all_gather(new_v.astype(jnp.bfloat16), "fs", axis=0, tiled=True),
        lax.all_gather(new_g.astype(jnp.bfloat16), "fs", axis=0, tiled=True),
        lax.all_gather(new_p.astype(jnp.bfloat16), "fs", axis=0, tiled=True),
    )
    return (new_v, new_g, new_p, copy_v, copy_g, copy_p, fv, fg, fpt, sv, sg, spt)


def solution(mesh):
    return jax.shard_map(
        local,
        mesh=mesh,
        in_specs=(
            P("fs", None),
            P("fs", "tp"),
            P("fs", "tp"),
            P("fs", None),
            P("fs", "tp"),
            P("fs", "tp"),
            P("fs", "tp"),
            P("fs", "tp"),
            P("fs", None),
            P("fs", None),
            P("fs", None),
            P("fs", "tp"),
            P("fs", "tp"),
            P("fs", "tp"),
            P("fs", "tp"),
            P("fs", "tp"),
            P("fs", "tp"),
        ),
        out_specs=(
            P("fs", "tp"),
            P("fs", "tp"),
            P("fs", "tp"),
            P(None, "tp"),
            P(None, "tp"),
            P(None, "tp"),
            P("fs", "tp"),
            P("fs", "tp"),
            P("fs", "tp"),
            P("fs", "tp"),
            P("fs", "tp"),
            P("fs", "tp"),
        ),
        check_vma=False,
    )
```

profile of v0, /device:TPU:0, one launch (start us, length us, event | category | flops | bytes accessed | tf_op | source)
XLA Modules:
  0.0 531.6 jit_solution(17776841322710641022)
XLA Ops:
  7.2 33.4 %all_gather.31 = bf16[1024,256]{1,0:T(8,128)(2,1)S(1)} all-gather(bf16[128,256]{1,0:T(8,128)(2,1)} %param.27), channel_id=1, replica_groups=mesh['fs'=8,'tp'=4] {'fs'}, dimensions={0}, use_global_device_ids=true | all-gather | bytes 589824 | tf_op jit(solution)/shard_map/all_gather | solution.py:59
  40.6 3.5 fusion.14
  47.6 61.6 %reduce-scatter.8.cloned.1.call-done = f32[32,256]{1,0:T(8,128)} async-done(((f32[256,256]{1,0:T(8,128)}), f32[32,256]{1,0:T(8,128)}) %reduce-scatter.8.cloned.1.call-update) | async-done | bytes 32784 | tf_op jit(solution)/shard_map/reduce_scatter | solution.py:68
  109.2 1.4 add_divide_fusion
  110.6 31.4 %all_gather.32 = f32[256,256]{1,0:T(8,128)S(1)} all-gather(f32[32,256]{1,0:T(8,128)S(1)} %get-tuple-element.33), channel_id=1, replica_groups=mesh['fs'=8,'tp'=4] {'fs'}, dimensions={0}, use_global_device_ids=true | all-gather | bytes 294912 | tf_op jit(solution)/shard_map/all_gather | solution.py:76
  142.0 18.3 %all-gather.7.cloned.1.call-done = bf16[4096,256]{1,0:T(8,128)(2,1)} async-done(((bf16[512,256]{1,0:T(8,128)(2,1)}), bf16[4096,256]{1,0:T(8,128)(2,1)}) %all-gather.7.cloned.1.call-update) | async-done | bytes 2097168 | tf_op jit(solution)/shard_map/all_gather | solution.py:53
  160.3 8.7 %fusion.13 = f32[2048,256]{1,0:T(8,128)S(1)} fusion(bf16[2048,4096]{1,0:T(8,128)(2,1)} %param.17, bf16[4096,256]{1,0:T(8,128)(2,1)} %all-gather.7.cloned.1.call-done), kind=kOutput, calls=%fused_computation.34 | convolution fusion | flops 4294967296 | bytes 20971520 | tf_op jit(solution)/shard_map/dot_general | solution.py:51
  169.5 1.2 convolution_add_fusion.1
  170.8 39.5 %all-gather.5.cloned.1.call-done = bf16[4096,256]{1,0:T(8,128)(2,1)} async-done(((bf16[512,256]{1,0:T(8,128)(2,1)}), bf16[4096,256]{1,0:T(8,128)(2,1)}) %all-gather.5.cloned.1.call-update) | async-done | bytes 2097168 | tf_op jit(solution)/shard_map/all_gather | solution.py:48
  210.3 8.7 %fusion.12 = f32[2048,256]{1,0:T(8,128)S(1)} fusion(bf16[2048,4096]{1,0:T(8,128)(2,1)} %param.17, bf16[4096,256]{1,0:T(8,128)(2,1)} %all-gather.5.cloned.1.call-done), kind=kOutput, calls=%fused_computation.33 | convolution fusion | flops 4294967296 | bytes 20971520 | tf_op jit(solution)/shard_map/dot_general | solution.py:46
  219.6 1.2 convolution_add_fusion.2
  221.8 52.9 %reduce-scatter.6.cloned.1.call-done = f32[32,256]{1,0:T(8,128)} async-done(((f32[256,256]{1,0:T(8,128)}), f32[32,256]{1,0:T(8,128)}) %reduce-scatter.6.cloned.1.call-update) | async-done | bytes 32784 | tf_op jit(solution)/shard_map/reduce_scatter | solution.py:67
  274.7 1.4 add_divide_fusion.1
  276.1 30.9 %all_gather.30 = f32[256,256]{1,0:T(8,128)S(1)} all-gather(f32[32,256]{1,0:T(8,128)S(1)} %get-tuple-element.36), channel_id=1, replica_groups=mesh['fs'=8,'tp'=4] {'fs'}, dimensions={0}, use_global_device_ids=true | all-gather | bytes 294912 | tf_op jit(solution)/shard_map/all_gather | solution.py:75
  307.1 32.6 %reduce-scatter.4.cloned.1.call-done = f32[32,256]{1,0:T(8,128)} async-done(((f32[256,256]{1,0:T(8,128)}), f32[32,256]{1,0:T(8,128)}) %reduce-scatter.4.cloned.1.call-update) | async-done | bytes 32784 | tf_op jit(solution)/shard_map/reduce_scatter | solution.py:66
  339.6 1.4 add_divide_fusion.2
  341.0 30.8 %all_gather.28 = f32[256,256]{1,0:T(8,128)S(1)} all-gather(f32[32,256]{1,0:T(8,128)S(1)} %get-tuple-element.39), channel_id=1, replica_groups=mesh['fs'=8,'tp'=4] {'fs'}, dimensions={0}, use_global_device_ids=true | all-gather | bytes 294912 | tf_op jit(solution)/shard_map/all_gather | solution.py:74
  374.3 38.0 %all-reduce = (f32[]{:T(128)}, f32[]{:T(128)}, f32[]{:T(128)}) all-reduce(f32[]{:T(128)} %get-tuple-element.42, f32[]{:T(128)} %get-tuple-element.44, f32[]{:T(128)} %get-tuple-element.46), channel_id=1, replica_groups=mesh['fs'=8,'tp'=4] {'fs','tp'}, use_global_device_ids=true, to_apply=%region_2.0 | all-reduce | flops 3 | bytes 24 | tf_op jit(solution)/shard_map/psum | solution.py:81
  413.8 1.2 copy.30
  418.2 29.7 %all_gather.35 = bf16[1024,256]{0,1:T(8,128)(2,1)S(1)} all-gather(bf16[128,256]{0,1:T(8,128)(2,1)S(1)} %get-tuple-element.27), channel_id=1, replica_groups=mesh['fs'=8,'tp'=4] {'fs'}, dimensions={0}, use_global_device_ids=true | all-gather | bytes 589824 | tf_op jit(solution)/shard_map/all_gather | solution.py:93
  450.9 19.2 %all-gather.9.cloned.1.call-done = bf16[4096,256]{0,1:T(8,128)(2,1)} async-done(((bf16[512,256]{0,1:T(8,128)(2,1)}), bf16[4096,256]{0,1:T(8,128)(2,1)}) %all-gather.9.cloned.1.call-update) | async-done | bytes 2097168 | tf_op jit(solution)/shard_map/all_gather | solution.py:91
  470.1 4.1 copy.35
  474.2 46.5 %all-gather.11.cloned.1.call-done = bf16[4096,256]{0,1:T(8,128)(2,1)} async-done(((bf16[512,256]{0,1:T(8,128)(2,1)}), bf16[4096,256]{0,1:T(8,128)(2,1)}) %all-gather.11.cloned.1.call-update) | async-done | bytes 2097168 | tf_op jit(solution)/shard_map/all_gather | solution.py:92
  520.7 4.1 copy.36
  (58 shorter events, 13.6 us)
Async XLA Ops:
  7.2 36.9 %copy-start = (bf16[2048,256]{1,0:T(8,128)(2,1)S(1)}, bf16[2048,256]{1,0:T(8,128)(2,1)}, u32[]{:S(2)}) copy-start(bf16[2048,256]{1,0:T(8,128)(2,1)} %param.21) | copy-start | bytes 3145732
  7.2 102.0 %reduce-scatter.8.cloned.1.call-start = ((), (), s32[]{:S(2)}) async-start(), calls=%async_computation.7 | async-start | bytes 294912 | tf_op jit(solution)/shard_map/reduce_scatter | solution.py:68
  44.6 2.8 copy-start.5
  44.6 64.6 %copy-start.8 = (f32[32,256]{1,0:T(8,128)S(1)}, f32[32,256]{1,0:T(8,128)}, u32[]{:S(2)}) copy-start(f32[32,256]{1,0:T(8,128)} %param.33) | copy-start | bytes 98308
  44.6 64.6 %copy-start.9 = (f32[32,256]{1,0:T(8,128)S(1)}, f32[32,256]{1,0:T(8,128)}, u32[]{:S(2)}) copy-start(f32[32,256]{1,0:T(8,128)} %param.30) | copy-start | bytes 98308
  45.8 114.4 %all-gather.7.cloned.1.call-start = ((), (), s32[]{:S(2)}) async-start(), calls=%async_computation.5 | async-start | bytes 2359296 | tf_op jit(solution)/shard_map/all_gather | solution.py:53
  46.6 163.7 %all-gather.5.cloned.1.call-start = ((), (), s32[]{:S(2)}) async-start(), calls=%async_computation.3 | async-start | bytes 2359296 | tf_op jit(solution)/shard_map/all_gather | solution.py:48
  47.3 227.4 %reduce-scatter.6.cloned.1.call-start = ((), (), s32[]{:S(2)}) async-start(), calls=%async_computation.6 | async-start | bytes 294912 | tf_op jit(solution)/shard_map/reduce_scatter | solution.py:67
  142.0 27.0 %copy-start.1 = (bf16[2048,256]{1,0:T(8,128)(2,1)S(1)}, bf16[2048,256]{1,0:T(8,128)(2,1)}, u32[]{:S(2)}) copy-start(bf16[2048,256]{1,0:T(8,128)(2,1)} %param.19) | copy-start | bytes 3145732
  170.7 48.2 %copy-start.2 = (bf16[2048,256]{1,0:T(8,128)(2,1)S(1)}, bf16[2048,256]{1,0:T(8,128)(2,1)}, u32[]{:S(2)}) copy-start(bf16[2048,256]{1,0:T(8,128)(2,1)} %param.18) | copy-start | bytes 3145732
  170.7 168.9 %reduce-scatter.4.cloned.1.call-start = ((), (), s32[]{:S(2)}) async-start(), calls=%async_computation.4 | async-start | bytes 294912 | tf_op jit(solution)/shard_map/reduce_scatter | solution.py:66
  219.5 1.4 copy-start.6
  219.5 55.2 %copy-start.10 = (f32[32,256]{1,0:T(8,128)S(1)}, f32[32,256]{1,0:T(8,128)}, u32[]{:S(2)}) copy-start(f32[32,256]{1,0:T(8,128)} %param.32) | copy-start | bytes 98308
  219.5 55.2 %copy-start.11 = (f32[32,256]{1,0:T(8,128)S(1)}, f32[32,256]{1,0:T(8,128)}, u32[]{:S(2)}) copy-start(f32[32,256]{1,0:T(8,128)} %param.29) | copy-start | bytes 98308
  219.5 120.1 %copy-start.12 = (f32[32,256]{1,0:T(8,128)S(1)}, f32[32,256]{1,0:T(8,128)}, u32[]{:S(2)}) copy-start(f32[32,256]{1,0:T(8,128)} %param.31) | copy-start | bytes 98308
  219.5 120.1 %copy-start.13 = (f32[32,256]{1,0:T(8,128)S(1)}, f32[32,256]{1,0:T(8,128)}, u32[]{:S(2)}) copy-start(f32[32,256]{1,0:T(8,128)} %param.28) | copy-start | bytes 98308
  219.6 152.3 %copy-start.3 = (bf16[512,256]{1,0:T(8,128)(2,1)S(1)}, bf16[512,256]{1,0:T(8,128)(2,1)}, u32[]{:S(2)}) copy-start(bf16[512,256]{1,0:T(8,128)(2,1)} %param.25) | copy-start | bytes 786436
  220.8 152.3 %copy-start.4 = (bf16[512,256]{1,0:T(8,128)(2,1)S(1)}, bf16[512,256]{1,0:T(8,128)(2,1)}, u32[]{:S(2)}) copy-start(bf16[512,256]{1,0:T(8,128)(2,1)} %param.26) | copy-start | bytes 786436
  220.8 249.3 %all-gather.9.cloned.1.call-start = ((), (), s32[]{:S(2)}) async-start(), calls=%async_computation.8 | async-start | bytes 2359296 | tf_op jit(solution)/shard_map/all_gather | solution.py:91
  413.7 2.9 copy-start.7
  413.8 106.9 %all-gather.11.cloned.1.call-start = ((), (), s32[]{:S(2)}) async-start(), calls=%async_computation.9 | async-start | bytes 2359296 | tf_op jit(solution)/shard_map/all_gather | solution.py:92
Sparse Core Ops, SparseCore 0:
  46.0 63.1 reduce-scatter.7
  111.3 48.9 all-gather.6
  162.4 47.8 all-gather.4
  214.0 60.6 reduce-scatter.5
  278.5 61.1 reduce-scatter.3
  413.9 56.1 all-gather.8
  472.1 48.5 all-gather.10
where the time goes:
time: 532 us
  waiting for transfers between devices  272 us (51%)
  blocking collectives  194 us (36%)
  matrix products  29.3 us (6%)
  between operations  16.4 us (3%)
  local copies, waits for them, and re-layouts  13.5 us (3%)
  other arithmetic  5.86 us (1%)
    reduce_scatter x1, waiting for transfers between devices, local(): lax.psum_scatter(low_point, 'fs', scatter_dimension=0, tiled=True)  61.6 us
    reduce_scatter x1, waiting for transfers between devices, local(): lax.psum_scatter(low_gate, 'fs', scatter_dimension=0, tiled=True)  52.9 us
    all_gather x1, waiting for transfers between devices, local(): lax.all_gather(new_g.astype(jnp.bfloat16), 'fs', axis=0, tiled=True)  46.5 us
    all_gather x1, waiting for transfers between devices, local(): lax.all_gather(factor_value, 'fs', axis=0, tiled=True)  39.5 us
    psum x1, blocking collectives, local(): lax.psum((jnp.sum(full_v * full_v), jnp.sum(full_g * full_g), jnp.sum(ful...  38 us
    all_gather x1, blocking collectives, local(): lax.all_gather(factor_point, 'fs', axis=0, tiled=True)  33.4 us
    reduce_scatter x1, waiting for transfers between devices, local(): lax.psum_scatter(low_value, 'fs', scatter_dimension=0, tiled=True)  32.6 us
    all_gather x1, blocking collectives, local(): lax.all_gather(dpt, 'fs', axis=0, tiled=True)  31.4 us
  transfers between devices with their start and end apart: 7, of which 7 were waited for; matrix products, arithmetic and copies ran while one was open for 7% of the time, Pallas kernels for 0%

commit v1 on v0

v1 whole, which is shorter than its diff:
```python
import functools

import jax
import jax.numpy as jnp
from jax import lax
from jax.experimental import pallas as pl
from jax.experimental.pallas import tpu as pltpu
from jax.sharding import PartitionSpec as P

MESH = pl.DeviceIdType.MESH
F32 = jnp.float32
BF16 = jnp.bfloat16


def tile_of(total, most):
    size = min(total, most)
    while total % size:
        size -= 8
    return size


def ring_position(index, n):
    half, odd = index // 2, index % 2
    return half + odd * (n - 1 - 2 * half)


def ring_index(position, n):
    back = position // (n // 2)
    return 2 * (position + back * (n - 1 - 2 * position)) + back


class Plan:
    def __init__(self, send, recv):
        self.send, self.recv, self.names, self.sent = send, recv, {}, []

    def copy(self, name, src, dst, device):
        slot = self.names.setdefault(name, len(self.names))
        return pltpu.make_async_remote_copy(
            src_ref=src, dst_ref=dst, send_sem=self.send.at[slot], recv_sem=self.recv.at[slot],
            device_id=device, device_id_type=MESH,
        )

    def start(self, name, src, dst, device):
        copy = self.copy(name, src, dst, device)
        copy.start()
        self.sent.append(copy)

    def arrived(self, name, dst, device):
        self.copy(name, dst, dst, device).wait_recv()

    def drain(self):
        for copy in self.sent:
            copy.wait_send()


def kernel(
    n, m, splits,
    x, xp, yv, yg, yp, mv, mg, mp, fv, fg, fp,
    f0, f1, f2, s0, s1, s2,
    out_pv, out_pg, out_pp, out_mv, out_mg, out_mp, out_low, out_dir, out_ss,
    xbuf, xpbuf, ybuf, vg, pp, mvg, mpp, m32, mp32, acc, lows, low_send, low_recv, dir_all, ss_own, ss_all,
    send, recv, local,
):
    fs, tp = lax.axis_index("fs"), lax.axis_index("tp")
    here = ring_position(fs, n)
    right = {"fs": ring_index((here + 1) % n, n)}
    left = {"fs": ring_index((here + n - 1) % n, n)}
    pairs = m // 2
    q, c = tp // 2, tp % 2
    partner = {"tp": 2 * q + 1 - c}
    rows, rows_p = fv.shape[0], fp.shape[0]
    tokens = x.shape[0]
    rank = vg.shape[2]
    part = rank // n
    half = n // 2
    net = Plan(send, recv)
    slots = iter(range(local.shape[0]))

    def fetch(src, dst):
        copy = pltpu.make_async_copy(src, dst, local.at[next(slots)])
        copy.start()
        return copy

    def block(event):
        if event == 0:
            return fs
        step = (event + 1) // 2
        return ring_index((here + (n - step if event % 2 else step)) % n, n)

    blocks = [block(e) for e in range(n)]

    def span(start, size, align):
        return pl.ds(pl.multiple_of(start, align), size)

    own = span(fs * rows, rows, rows)
    own_p = span(fs * rows_p, rows_p, rows_p)
    factor_in = [
        fetch(fp, pp.at[own_p]), fetch(fv, vg.at[0, own]), fetch(fg, vg.at[1, own]),
    ]
    master_in = [fetch(mv, m32.at[0]), fetch(mg, m32.at[1]), fetch(mp, mp32)]
    x_in = []
    for e in range(n):
        x_in.append(fetch(x.at[:, span(blocks[e] * rows, rows, rows)], xbuf.at[e]))
        if e == 0:
            xp_in = fetch(xp, xpbuf)
    y_in = [fetch(yv, ybuf.at[0]), fetch(yg, ybuf.at[1]), fetch(yp, ybuf.at[2])]

    barrier = pltpu.get_barrier_semaphore()
    for d in range(1, n):
        pl.semaphore_signal(barrier, inc=1, device_id={"fs": (fs + d) % n}, device_id_type=MESH)
    for d in range(1, m):
        pl.semaphore_signal(barrier, inc=1, device_id={"tp": (tp + d) % m}, device_id_type=MESH)
    for copy in factor_in:
        copy.wait()
    pl.semaphore_wait(barrier, n - 1 + m - 1)

    def piece(ref, owner, lo, size, align):
        if len(ref.shape) == 3:
            return ref.at[:, span(owner, size, align)] if lo is None else ref.at[:, span(owner + lo, size, align)]
        return ref.at[span(owner, size, align)] if lo is None else ref.at[span(owner + lo, size, align)]

    def stream(name, ref, size, split):
        sent = size // split
        offset = 0 if split == 1 else tp * sent
        return (name, ref, size, offset, sent)

    factors = [stream("p", pp, rows_p, splits[1]), stream("vg", vg, rows, splits[0])]
    masters = [stream("mvg", mvg, rows, 1), stream("mp", mpp, rows_p, 1)]

    def ring_piece(item, event, way):
        name, ref, size, offset, sent = item
        last = event == n - 1
        if last:
            cut = sent // 2
            return piece(ref, blocks[event] * size + offset + way * cut, None, cut, cut)
        return piece(ref, blocks[event] * size + offset, None, sent, sent)

    def ring_send(item, step):
        for way, device in ((0, right), (1, left)):
            event = 0 if step == 1 else 2 * (step - 1) - 1 + way
            name, ref, size, offset, sent = item
            base = blocks[event] * size + offset
            if step == half:
                cut = sent // 2
                part_ref = piece(ref, base + way * cut, None, cut, cut)
            else:
                part_ref = piece(ref, base, None, sent, sent)
            net.start((name, way, step), part_ref, part_ref, device)

    def ring_wait(item, step):
        for way, device in ((0, right), (1, left)):
            event = n - 1 if step == half else 2 * step - 1 + way
            net.arrived((item[0], way, step), ring_piece(item, event, way), device)

    def events_of(step):
        if step == 0:
            return [0]
        return [n - 1] if step == half else [2 * step - 1, 2 * step]

    def quarter(item, event, holder):
        name, ref, size, offset, sent = item
        return piece(ref, blocks[event] * size + holder * sent, None, sent, sent)

    split_items = [item for item, s in zip(factors, (splits[1], splits[0])) if s > 1]

    def share(step):
        for e in events_of(step) if step else []:
            for item in split_items:
                mine = quarter(item, e, tp)
                for d in range(1, pairs):
                    net.start((item[0], "x", d, e), mine, mine, {"tp": 2 * ((q + d) % pairs) + c})
                net.start((item[0], "c", 0, e), mine, mine, partner)

    def relay(step):
        for e in events_of(step) if step else []:
            for item in split_items:
                for d in range(1, pairs):
                    other = quarter(item, e, 2 * ((q + pairs - d) % pairs) + c)
                    net.arrived((item[0], "x", d, e), other, partner)
                    net.start((item[0], "c", d, e), other, other, partner)

    def gathered(step):
        for e in events_of(step) if step else []:
            for item in split_items:
                for d in range(pairs):
                    other = quarter(item, e, 2 * ((q + pairs - d) % pairs) + 1 - c)
                    net.arrived((item[0], "c", d, e), other, partner)

    tile = tile_of(tokens, 512)

    def project(step):
        for e in events_of(step):
            x_in[e].wait()
            at = span(blocks[e] * rows, rows, rows)

            def body(i, carry, e=e, at=at):
                r = span(i * tile, tile, tile)
                left_side = xbuf[e, r]
                for a in range(2):
                    got = jnp.dot(left_side, vg[a, at], preferred_element_type=F32)
                    if e == 0:
                        acc[a, r] = got
                    else:
                        acc[a, r] += got
                return carry

            lax.fori_loop(0, tokens // tile, body, 0)

    def project_point():
        xp_in.wait()

        def body(i, carry):
            r = span(i * tile, tile, tile)
            acc[2, r] = jnp.dot(xpbuf[r], pp[...], preferred_element_type=F32)
            return carry

        lax.fori_loop(0, tokens // tile, body, 0)

    outs = []

    def master_stage(step):
        for item in masters:
            ring_wait(item, step)
            if step < half:
                ring_send(item, step + 1)
        store_master(step)

    def store_master(step):
        for e in events_of(step):
            b, bp = span(blocks[e] * rows, rows, rows), span(blocks[e] * rows_p, rows_p, rows_p)
            outs.append(fetch(mvg.at[0, b], out_mv.at[b]))
            outs.append(fetch(mvg.at[1, b], out_mg.at[b]))
            outs.append(fetch(mpp.at[bp], out_mp.at[bp]))

    def master_first():
        for copy in master_in:
            copy.wait()
        mvg[0, own] = m32[0].astype(BF16)
        mvg[1, own] = m32[1].astype(BF16)
        mpp[own_p] = mp32[...].astype(BF16)

    for item in factors:
        ring_send(item, 1)
    share(0)
    master_first()
    project(0)
    for step in range(1, half + 1):
        for item in factors:
            ring_wait(item, step)
            if step < half:
                ring_send(item, step + 1)
        share(step)
        if step == half - 1:
            for item in masters:
                ring_send(item, 1)
            store_master(0)
        relay(step - 1)
        if step >= 3:
            gathered(step - 2)
            project(step - 2)
    relay(half)
    gathered(half - 1)
    project(half - 1)
    gathered(half)
    project(half)
    project_point()
    outs.append(fetch(vg.at[0], out_pv))
    outs.append(fetch(vg.at[1], out_pg))
    outs.append(fetch(pp, out_pp))

    for copy in y_in:
        copy.wait()
    lows[...] = jnp.zeros_like(lows)

    def contract(i, carry):
        r = span(i * tile, tile, tile)
        for a in range(3):
            value = acc[a, r]
            upper = value.astype(BF16)
            lower = (value - upper.astype(F32)).astype(BF16)
            cot = ybuf[a, r]
            dims = (((0,), (0,)), ((), ()))
            lows[a] += lax.dot_general(
                upper, cot, dims, preferred_element_type=F32
            ) + lax.dot_general(lower, cot, dims, preferred_element_type=F32)
        return carry

    lax.fori_loop(0, tokens // tile, contract, 0)
    for a in range(3):
        for b in range(n):
            low_send[b, a] = (lows[a, b * part : (b + 1) * part] / (tokens * n)).astype(BF16)
    for d in range(1, n):
        to = (fs + d) % n
        net.start(("low", d), low_send.at[to], low_recv.at[fs], {"fs": to})
    master_stage(1)
    mine = span(fs * part, part, part)
    for d in range(1, n):
        src = (fs + n - d) % n
        net.arrived(("low", d), low_recv.at[src], {"fs": src})
    for a, (first_old, second_old) in enumerate(((f0, s0), (f1, s1), (f2, s2))):
        low = lows[a, mine] / (tokens * n)
        for d in range(1, n):
            low = low + low_recv[(fs + d) % n, a].astype(F32)
        out_low[a] = low
        first = 0.8 * first_old[...] + 0.2 * low
        second = 0.9 * second_old[...] + 0.1 * low * low
        dir_all[fs, a] = (first / (jnp.sqrt(second) + 1e-08)).astype(BF16)
    for d in range(1, n):
        to = (fs + d) % n
        net.start(("dir", d), dir_all.at[fs], dir_all.at[fs], {"fs": to})
    if half >= 3:
        master_stage(2)
    for d in range(1, n):
        src = (fs + n - d) % n
        net.arrived(("dir", d), dir_all.at[src], {"fs": src})
    sums = []
    for a in range(3):
        whole = jnp.concatenate([dir_all[b, a].astype(F32) for b in range(n)], axis=0)
        out_dir[a] = whole.astype(BF16)
        size = rows if a < 2 else rows_p

        def square(i, total, a=a, size=size):
            r = span(i * size, size, size)
            block_ref = vg[a, r] if a < 2 else pp[r]
            full = jnp.dot(block_ref, out_dir[a], preferred_element_type=F32)
            return total + jnp.sum(full * full, axis=0, keepdims=True)

        total = lax.fori_loop(0, n, square, jnp.zeros((1, out_dir.shape[2]), F32))
        sums.append(jnp.sum(total, axis=1, keepdims=True))
    row = lax.broadcasted_iota(jnp.int32, ss_own.shape, 0)
    ss_own[...] = jnp.where(row == 0, sums[0], jnp.where(row == 1, sums[1], sums[2]))
    for d in range(1, m):
        net.start(("ss", d), ss_own, ss_all.at[tp], {"tp": (tp + d) % m})
    ss_all[tp] = ss_own[...]
    for d in range(1, m):
        src = (tp + m - d) % m
        net.arrived(("ss", d), ss_all.at[src], {"tp": src})
    total = ss_all[0]
    for t in range(1, m):
        total = total + ss_all[t]
    out_ss[...] = total
    for step in range(3 if half >= 3 else 2, half + 1):
        master_stage(step)
    net.drain()
    for copy in outs:
        copy.wait()


def finish(entries, *refs):
    whole, held, master, factor = refs[0:3], refs[3:6], refs[6:9], refs[9:12]
    low, direction, squares = refs[12:15]
    olds, outs = refs[15:21], refs[21:]
    for a in range(3):
        step = 0.1 * lax.rsqrt(squares[a : a + 1, 0:1] / entries[a] + 1e-06)
        own = jnp.dot(factor[a][...], direction[a], preferred_element_type=F32)
        outs[a][...] = master[a][...] - step * own
        full = jnp.dot(whole[a][...], direction[a], preferred_element_type=F32)
        outs[3 + a][...] = (held[a][...].astype(F32) - step * full).astype(BF16)

    @pl.when(pl.program_id(0) == 0)
    def _():
        for a in range(3):
            outs[6 + a][...] = 0.8 * olds[a][...] + 0.2 * low[a]
            outs[9 + a][...] = 0.9 * olds[3 + a][...] + 0.1 * low[a] * low[a]


def local(n, m, *args):
    x, yv, yg, xp, yp, mv, mg, mp, fv, fg, fp, f0, f1, f2, s0, s1, s2 = args
    tokens = x.shape[0]
    rows, rows_p, rank, width = fv.shape[0], fp.shape[0], fv.shape[1], yv.shape[1]
    depth, depth_p, part = rows * n, rows_p * n, rank // n
    splits = tuple(m if r % (32 * m) == 0 else 1 for r in (rows, rows_p))
    half = n // 2
    shared = sum(s > 1 for s in splits)
    remote = 4 * 2 * half + shared * (n - 1) * (2 * (m // 2) - 1) + 2 * (n - 1) + m - 1
    any_spec, vmem = pl.BlockSpec(memory_space=pl.ANY), pl.BlockSpec(memory_space=pltpu.VMEM)
    shape = jax.ShapeDtypeStruct
    pv, pg, pp, bv, bg, bp, low, direction, squares = pl.pallas_call(
        functools.partial(kernel, n, m, splits),
        out_shape=(
            shape((depth, rank), BF16), shape((depth, rank), BF16), shape((depth_p, rank), BF16),
            shape((depth, width), BF16), shape((depth, width), BF16), shape((depth_p, width), BF16),
            shape((3, part, width), F32), shape((3, rank, width), BF16), shape((8, 128), F32),
        ),
        in_specs=[any_spec] * 11 + [vmem] * 6,
        out_specs=(any_spec,) * 6 + (vmem,) * 3,
        scratch_shapes=[
            pltpu.VMEM((n, tokens, rows), BF16),
            pltpu.VMEM(xp.shape, BF16),
            pltpu.VMEM((3, tokens, width), BF16),
            pltpu.VMEM((2, depth, rank), BF16),
            pltpu.VMEM((depth_p, rank), BF16),
            pltpu.VMEM((2, depth, width), BF16),
            pltpu.VMEM((depth_p, width), BF16),
            pltpu.VMEM((2, rows, width), F32),
            pltpu.VMEM((rows_p, width), F32),
            pltpu.VMEM((3, tokens, rank), F32),
            pltpu.VMEM((3, rank, width), F32),
            pltpu.VMEM((n, 3, part, width), BF16),
            pltpu.VMEM((n, 3, part, width), BF16),
            pltpu.VMEM((n, 3, part, width), BF16),
            pltpu.VMEM((8, 128), F32),
            pltpu.VMEM((m, 8, 128), F32),
            pltpu.SemaphoreType.DMA((remote,)),
            pltpu.SemaphoreType.DMA((remote,)),
            pltpu.SemaphoreType.DMA((3 + 3 + n + 1 + 3 + 3 + 3 * n,)),
        ],
        compiler_params=pltpu.CompilerParams(
            collective_id=0, has_side_effects=True, vmem_limit_bytes=67043328
        ),
    )(x, xp, yv, yg, yp, mv, mg, mp, fv, fg, fp, f0, f1, f2, s0, s1, s2)

    steps = 4
    entries = (depth * width * m, depth * width * m, depth_p * width * m)

    def by_rows(array):
        return pl.BlockSpec((array.shape[0] // steps, array.shape[1]), lambda i: (i, 0))

    def fixed(array):
        return pl.BlockSpec(array.shape, lambda i: (0,) * len(array.shape))

    streamed = (pv, pg, pp, bv, bg, bp, mv, mg, mp, fv, fg, fp)
    kept = (low, direction, squares, f0, f1, f2, s0, s1, s2)
    results = tuple(shape(a.shape, F32) for a in (mv, mg, mp)) + tuple(
        shape(a.shape, BF16) for a in (bv, bg, bp)
    )
    small = tuple(shape(a.shape, F32) for a in (f0, f1, f2, s0, s1, s2))
    return pl.pallas_call(
        functools.partial(finish, entries),
        grid=(steps,),
        out_shape=results + small,
        in_specs=[by_rows(a) for a in streamed] + [fixed(a) for a in kept],
        out_specs=tuple(by_rows(a) for a in results) + tuple(fixed(a) for a in small),
        compiler_params=pltpu.CompilerParams(vmem_limit_bytes=50000000),
    )(*streamed, *kept)


def solution(mesh):
    rows, both, cols = P("fs", None), P("fs", "tp"), P(None, "tp")
    return jax.shard_map(
        functools.partial(local, mesh.shape["fs"], mesh.shape["tp"]),
        mesh=mesh,
        in_specs=(rows, both, both, rows, both, both, both, both, rows, rows, rows) + (both,) * 6,
        out_specs=(both,) * 3 + (cols,) * 3 + (both,) * 6,
        check_vma=False,
    )
```

time: 532 us -> 123 us (0.23)
  waiting for transfers between devices: 272 us -> 0 us
  blocking collectives: 194 us -> 0 us
  Pallas kernels: 0 us -> 105 us
  matrix products: 29.3 us -> 0 us
  between operations: 16.4 us -> 0.68 us
  other arithmetic: 5.86 us -> 0 us
    all_gather x5 -> x0, blocking collectives: 156 us -> none  [the longest x1 33.4 us: local(): lax.all_gather(factor_point, 'fs', axis=0, tiled=True)]
    reduce_scatter x3 -> x0, waiting for transfers between devices: 147 us -> none  [the longest x1 61.6 us: local(): lax.psum_scatter(low_point, 'fs', scatter_dimension=0, tiled=True)]
    all_gather x4 -> x0, waiting for transfers between devices: 123 us -> none  [the longest x1 46.5 us: local(): lax.all_gather(new_g.astype(jnp.bfloat16), 'fs', axis=0, tiled=True)]
    pallas_call x0 -> x2, Pallas kernels: none -> 105 us  [the longest x1 97.9 us: local(): pl.pallas_call(functools.partial(kernel, n, m, splits), out_shape=(shape(...]
    psum x1 -> x0, blocking collectives: 38 us -> none  [local(): lax.psum((jnp.sum(full_v * full_v), jnp.sum(full_g * full_g), jnp.sum(ful...]
    dot_general x12 -> x0, matrix products: 29.3 us -> none  [the longest x1 8.72 us: local(): jnp.dot(columns, lax.all_gather(factor_gate, 'fs', axis=0, tiled=True), p...]
    unnamed x37 -> x36, local copies, waits for them, and re-layouts: 13.5 us -> 16.5 us
  transfers between devices with their start and end apart: 7 -> 0, of which waited for: 7 -> 0; matrix products, arithmetic and copies ran while one was open for 7% -> 0% of each run, Pallas kernels for 0% -> 0%
where the time goes in v1:
time: 123 us; the launch traced here: 122 us
  Pallas kernels  105 us (85%)
  local copies, waits for them, and re-layouts  16.5 us (13%)
    pallas_call x1, Pallas kernels, local(): pl.pallas_call(functools.partial(kernel, n, m, splits), out_shape=(shape(...  97.9 us
    unnamed x36, local copies, waits for them, and re-layouts  16.5 us
    pallas_call x1, Pallas kernels, local(): pl.pallas_call(functools.partial(finish, entries), grid=(steps,), out_sha...  6.66 us

profile of v1, /device:TPU:0, one launch (start us, length us, event | category | flops | bytes accessed | tf_op | source)
XLA Modules:
  0.0 121.7 jit_solution(10948509622508418399)
XLA Ops:
  0.6 97.9 %shard_map.256 = (bf16[4096,256]{1,0:T(8,128)(2,1)}, bf16[4096,256]{1,0:T(8,128)(2,1)}, bf16[1024,256]{1,0:T(8,128)(2,1)}, bf16[4096,256]{1,0:T(8,128)(2,1)}, bf...) custom-call(bf16[2048,4096]{1,0:T(8,128)(2,1)} %x.1, ...), custom_call_target="tpu_custom_call" | custom-call | tf_op jit(solution)/shard_map/pallas_call | solution.py:378
  98.5 0.0 copy-start
  98.5 1.0 copy-done
  99.6 0.0 copy-start.1
  99.6 1.0 copy-done.1
  100.6 0.0 copy-start.2
  100.6 1.6 %copy-done.2 = bf16[4096,256]{1,0:T(8,128)(2,1)S(1)} copy-done((bf16[4096,256]{1,0:T(8,128)(2,1)S(1)}, bf16[4096,256]{1,0:T(8,128)(2,1)}, u32[]{:S(2)}) %copy-start.2) | copy-done | bytes 2097176
  102.2 0.0 copy-start.3
  102.2 0.9 copy-done.3
  103.2 0.9 copy-done.4
  104.1 0.9 copy-done.5
  105.0 1.0 copy-done.6
  106.1 1.0 copy-done.7
  107.1 1.0 copy-done.8
  108.1 0.8 copy-done.9
  108.9 0.8 copy-done.10
  109.7 0.8 copy-done.11
  110.5 0.8 copy-done.12
  111.2 0.8 copy-done.13
  112.0 0.8 copy-done.14
  112.7 0.8 copy-done.15
  113.5 0.9 copy-done.16
  114.4 0.7 copy-done.17
  115.1 6.7 %shard_map.257 = (f32[512,256]{1,0:T(8,128)}, f32[512,256]{1,0:T(8,128)}, f32[128,256]{1,0:T(8,128)}, bf16[4096,256]{1,0:T(8,128)(2,1)}, bf16[4096,256]{1,0:T(8,...) custom-call(bf16[4096,256]{1,0:T(8,128)(2,1)S(1)} %copy-done.2, ...), custom_call_target="tpu_custom_call" | custom-call | tf_op jit(solution)/shard_map/pallas_call | solution.py:428
  (14 shorter events, 0.0 us)
Async XLA Ops:
  98.5 1.0 copy-start
  99.6 1.0 copy-start.1
  100.6 1.6 %copy-start.2 = (bf16[4096,256]{1,0:T(8,128)(2,1)S(1)}, bf16[4096,256]{1,0:T(8,128)(2,1)}, u32[]{:S(2)}) copy-start(bf16[4096,256]{1,0:T(8,128)(2,1)} %get-tuple-element.21.refs_0_) | copy-start | bytes 6291460
  102.2 0.9 copy-start.3
  103.2 0.9 copy-start.4
  104.1 0.9 copy-start.5
  105.0 1.0 copy-start.6
  106.1 1.0 copy-start.7
  107.1 1.0 copy-start.8
  108.1 0.8 copy-start.9
  108.9 0.8 copy-start.10
  109.7 0.8 copy-start.11
  110.5 0.8 copy-start.12
  111.2 0.8 copy-start.13
  112.0 0.8 copy-start.14
  112.7 0.8 copy-start.15
  113.5 0.9 copy-start.16
  114.4 0.7 copy-start.17

commit v2 on v1

--- a/solution.py
+++ b/solution.py
@@ -262,6 +262,7 @@
     gathered(half - 1)
     project(half - 1)
     gathered(half)
+    master_stage(1)
     project(half)
     project_point()
     outs.append(fetch(vg.at[0], out_pv))
@@ -292,7 +293,6 @@
     for d in range(1, n):
         to = (fs + d) % n
         net.start(("low", d), low_send.at[to], low_recv.at[fs], {"fs": to})
-    master_stage(1)
     mine = span(fs * part, part, part)
     for d in range(1, n):
         src = (fs + n - d) % n
@@ -431,7 +431,7 @@
         out_shape=results + small,
         in_specs=[by_rows(a) for a in streamed] + [fixed(a) for a in kept],
         out_specs=tuple(by_rows(a) for a in results) + tuple(fixed(a) for a in small),
-        compiler_params=pltpu.CompilerParams(vmem_limit_bytes=50000000),
+        compiler_params=pltpu.CompilerParams(vmem_limit_bytes=67043328),
     )(*streamed, *kept)
 
 

time: 123 us -> 102 us (0.83)
  local copies, waits for them, and re-layouts: 16.5 us -> 0 us
  Pallas kernels: 105 us -> 100 us
    unnamed x36 -> x0, local copies, waits for them, and re-layouts: 16.5 us -> none
    pallas_call x1, Pallas kernels: 97.9 us -> 92.1 us  [local(): pl.pallas_call(functools.partial(kernel, n, m, splits), out_shape=(shape(...]
    pallas_call x1, Pallas kernels: 6.66 us -> 8.39 us  [local(): pl.pallas_call(functools.partial(finish, entries), grid=(steps,), out_sha...]
where the time goes in v2:
time: 102 us; the launch traced here: 101 us
  Pallas kernels  100 us (98%)
    pallas_call x1, Pallas kernels, local(): pl.pallas_call(functools.partial(kernel, n, m, splits), out_shape=(shape(...  92.1 us
    pallas_call x1, Pallas kernels, local(): pl.pallas_call(functools.partial(finish, entries), grid=(steps,), out_sha...  8.39 us

profile of v2, /device:TPU:0, one launch (start us, length us, event | category | flops | bytes accessed | tf_op | source)
XLA Modules:
  0.0 101.1 jit_solution(5429976893865014241)
XLA Ops:
  0.6 92.1 %shard_map.256 = (bf16[4096,256]{1,0:T(8,128)(2,1)}, bf16[4096,256]{1,0:T(8,128)(2,1)}, bf16[1024,256]{1,0:T(8,128)(2,1)}, bf16[4096,256]{1,0:T(8,128)(2,1)}, bf...) custom-call(bf16[2048,4096]{1,0:T(8,128)(2,1)} %x.1, ...), custom_call_target="tpu_custom_call" | custom-call | tf_op jit(solution)/shard_map/pallas_call | solution.py:378
  92.7 8.4 %shard_map.257 = (f32[512,256]{1,0:T(8,128)}, f32[512,256]{1,0:T(8,128)}, f32[128,256]{1,0:T(8,128)}, bf16[4096,256]{1,0:T(8,128)(2,1)}, bf16[4096,256]{1,0:T(8,...) custom-call(bf16[4096,256]{1,0:T(8,128)(2,1)} %get-tuple-element.21., ...), custom_call_target="tpu_custom_call" | custom-call | tf_op jit(solution)/shard_map/pallas_call | solution.py:428
